TPU v7x, 32 devices: a whole 2x2x4 slice. The times are simulated.
32 devices in a mesh: ep: 32 (over z, y, x, core).
Axes of the slice: x: 2, y: 2, z: 4, core: 2. Of those that a mesh axis runs over, the one named last changes fastest.
Arguments:
- tokens: bfloat16 [768, 2048], P('ep'), may hold values from -6 to 6
- lengths: int32 [768], P('ep'), may hold values from 2 to 1024
- latent_cache: bfloat16 [768, 1024, 256], P('ep'), may hold values from -500 to 500
- rotary_cache: bfloat16 [768, 1024, 32], P('ep'), may hold values from -6 to 6
- route_ids: int32 [768, 6], P('ep'), may hold values from 0 to 31, all different within a row; in each aligned block of 24 rows (0 to 23, 24 to 47, ...) at most 12 rows name the same one
- route_scores: float32 [768, 6], P('ep'), may hold values from 0.05 to 1
- attn_gain: bfloat16 [2048], replicated, may hold values from 0.099609375 to 1.8984375
- w_query_down: bfloat16 [2048, 256], replicated, may hold values from -0.125 to 0.125
- query_gain: bfloat16 [256], replicated, may hold values from 0.099609375 to 1.8984375
- w_query_nope: bfloat16 [256, 2048], replicated, may hold values from -0.375 to 0.375
- w_query_rope: bfloat16 [256, 1024], replicated, may hold values from -0.375 to 0.375
- w_key_absorb: bfloat16 [32, 64, 256], replicated, may hold values from -0.75 to 0.75
- latent_gain: bfloat16 [256], replicated, may hold values from 0.099609375 to 1.8984375
- w_latent_down: bfloat16 [2048, 256], replicated, may hold values from -0.125 to 0.125
- w_rotary_key: bfloat16 [2048, 32], replicated, may hold values from -0.125 to 0.125
- w_value_up: bfloat16 [32, 256, 64], replicated, may hold values from -0.375 to 0.375
- w_output: bfloat16 [2048, 2048], P(None, 'ep'), may hold values from -0.125 to 0.125
- ffn_gain: bfloat16 [2048], replicated, may hold values from 0.099609375 to 1.8984375
- expert_gate: bfloat16 [32, 2048, 512], P('ep'), may hold values from -0.125 to 0.125
- expert_up: bfloat16 [32, 2048, 512], P('ep'), may hold values from -0.125 to 0.125
- expert_down: bfloat16 [32, 512, 2048], P('ep'), may hold values from -0.25 to 0.25
- shared_gate: bfloat16 [2048, 256], replicated, may hold values from -0.125 to 0.125
- shared_up: bfloat16 [2048, 256], replicated, may hold values from -0.125 to 0.125
- shared_down: bfloat16 [256, 2048], replicated, may hold values from -0.375 to 0.375
Outputs:
- mixed: bfloat16 [768, 2048], P('ep')
- latent_new: bfloat16 [768, 256], P('ep')
- rotary_new: bfloat16 [768, 32], P('ep')
Inputs may be any that keep to these rules, and one draw needn't show every extreme that they name: `route_ids`: within the rows of one device no expert is named by more than 12 rows, a bound that some block reaches; each row names 6 different experts. `lengths`: cache positions at or past a sequence's length are not read.
All inputs are finite; a program needn't handle non-finite values.
Results may differ from a plain program's by a relative error of at most 0.025.
Values may be sent and summed in bfloat16 or wider, within the bound.
A program may use at most 128 MiB of HBM per device.

v0:
```python
import jax
import jax.numpy as jnp
from jax import lax
from jax.sharding import PartitionSpec as P

EPSILON = 1e-06
THETA = 10000.0
ROUTED_SCALE = 2.5


def rms_scale(values, gain):
    squares = jnp.mean(values * values, axis=-1, keepdims=True)
    return values * lax.rsqrt(squares + EPSILON) * gain.astype(jnp.float32)


def rotate(values, positions):
    half = values.shape[-1] // 2
    freqs = 1.0 / THETA ** (jnp.arange(half, dtype=jnp.float32) * 2.0 / values.shape[-1])
    angles = positions.astype(jnp.float32)[:, None] * freqs[None, :]
    if values.ndim == 3:
        angles = angles[:, None, :]
    cosine, sine = (jnp.cos(angles), jnp.sin(angles))
    first, second = (values[..., :half], values[..., half:])
    return jnp.concatenate(
        [first * cosine - second * sine, second * cosine + first * sine], axis=-1
    )


def shards(
    tokens,
    lengths,
    latent_cache,
    rotary_cache,
    route_ids,
    route_scores,
    attn_gain,
    w_query_down,
    query_gain,
    w_query_nope,
    w_query_rope,
    w_key_absorb,
    latent_gain,
    w_latent_down,
    w_rotary_key,
    w_value_up,
    w_output,
    ffn_gain,
    expert_gate,
    expert_up,
    expert_down,
    shared_gate,
    shared_up,
    shared_down,
):
    f32 = jnp.float32
    bf16 = jnp.bfloat16
    rows, model = tokens.shape
    heads, nope, latent = w_key_absorb.shape
    rotary = w_rotary_key.shape[1]
    top = route_ids.shape[1]
    normed = rms_scale(tokens.astype(f32), attn_gain).astype(bf16)
    query_low = rms_scale(
        jnp.dot(normed, w_query_down, preferred_element_type=f32), query_gain
    ).astype(bf16)
    query_nope = (
        jnp.dot(query_low, w_query_nope, preferred_element_type=f32)
        .astype(bf16)
        .reshape(rows, heads, nope)
    )
    query_rot = jnp.dot(query_low, w_query_rope, preferred_element_type=f32).reshape(
        rows, heads, rotary
    )
    query_rot = rotate(query_rot, lengths).astype(bf16)
    query_lat = jnp.einsum(
        "thn,hnl->thl", query_nope, w_key_absorb, preferred_element_type=f32
    ).astype(bf16)
    latent_new = rms_scale(
        jnp.dot(normed, w_latent_down, preferred_element_type=f32), latent_gain
    ).astype(bf16)
    rotary_new = rotate(jnp.dot(normed, w_rotary_key, preferred_element_type=f32), lengths).astype(
        bf16
    )
    scale = (nope + rotary) ** (-0.5)
    scores = (
        jnp.einsum("thl,tkl->thk", query_lat, latent_cache, preferred_element_type=f32)
        + jnp.einsum("thr,tkr->thk", query_rot, rotary_cache, preferred_element_type=f32)
    ) * scale
    live = jnp.arange(latent_cache.shape[1], dtype=jnp.int32)[None, :] < lengths[:, None]
    scores = jnp.where(live[:, None, :], scores, -jnp.inf)
    own = (
        jnp.einsum("thl,tl->th", query_lat, latent_new, preferred_element_type=f32)
        + jnp.einsum("thr,tr->th", query_rot, rotary_new, preferred_element_type=f32)
    ) * scale
    highest = jnp.maximum(jnp.max(scores, axis=-1), own)
    weights = jnp.exp(scores - highest[..., None])
    own_weight = jnp.exp(own - highest)
    total = jnp.sum(weights, axis=-1) + own_weight
    probs = (weights / total[..., None]).astype(bf16)
    own_prob = (own_weight / total).astype(bf16)
    out_lat = jnp.einsum("thk,tkl->thl", probs, latent_cache, preferred_element_type=f32)
    out_lat = (
        out_lat + own_prob.astype(f32)[..., None] * latent_new.astype(f32)[:, None, :]
    ).astype(bf16)
    values = jnp.einsum("thl,hlv->thv", out_lat, w_value_up, preferred_element_type=f32).astype(
        bf16
    )
    values = values.reshape(rows, model)
    attended = jnp.dot(
        values, lax.all_gather(w_output, "ep", axis=1, tiled=True), preferred_element_type=f32
    ).astype(bf16)
    residual = (tokens.astype(f32) + attended.astype(f32)).astype(bf16)
    ffn_in = rms_scale(residual.astype(f32), ffn_gain).astype(bf16)
    devices = lax.axis_size("ep")
    local_experts = expert_gate.shape[0]
    experts = devices * local_experts
    capacity = max(2, rows * top * 8 // (3 * experts))
    flat_ids = route_ids.reshape(-1)
    hits = (flat_ids[:, None] == jnp.arange(experts, dtype=jnp.int32)[None, :]).astype(jnp.int32)
    earlier = jnp.cumsum(hits, axis=0) - hits
    slot = jnp.sum(earlier * hits, axis=1)
    target = flat_ids * capacity + slot
    slot_range = jnp.arange(experts * capacity, dtype=jnp.int32)
    per_token = jnp.any(
        slot_range[:, None, None] == target.reshape(rows, top)[None, :, :], axis=2
    ).astype(bf16)
    per_pair = (target[:, None] == slot_range[None, :]).astype(bf16)
    outgoing = (
        jnp.dot(per_token, ffn_in, preferred_element_type=f32)
        .astype(bf16)
        .reshape(experts, capacity, model)
    )
    arrived = lax.all_to_all(outgoing, "ep", split_axis=0, concat_axis=0, tiled=True)
    count = arrived.shape[1]
    grouped = arrived.reshape(devices, local_experts, count, model)
    gate = jnp.einsum("sjcd,jdf->sjcf", grouped, expert_gate, preferred_element_type=f32)
    upward = jnp.einsum("sjcd,jdf->sjcf", grouped, expert_up, preferred_element_type=f32)
    hidden = (jax.nn.silu(gate) * upward).astype(bf16)
    result = jnp.einsum("sjcf,jfd->sjcd", hidden, expert_down, preferred_element_type=f32).astype(
        bf16
    )
    returned = lax.all_to_all(
        result.reshape(devices * local_experts, count, model),
        "ep",
        split_axis=0,
        concat_axis=0,
        tiled=True,
    )
    picked = jnp.dot(
        per_pair, returned.reshape(experts * capacity, model), preferred_element_type=f32
    )
    route_weight = ROUTED_SCALE * route_scores / jnp.sum(route_scores, axis=1, keepdims=True)
    routed = jnp.sum(picked.reshape(rows, top, model) * route_weight[:, :, None], axis=1)
    gate_shared = jnp.dot(ffn_in, shared_gate, preferred_element_type=f32)
    up_shared = jnp.dot(ffn_in, shared_up, preferred_element_type=f32)
    hidden_shared = (jax.nn.silu(gate_shared) * up_shared).astype(bf16)
    shared_out = jnp.dot(hidden_shared, shared_down, preferred_element_type=f32)
    mixed = (residual.astype(f32) + routed + shared_out).astype(bf16)
    return (mixed, latent_new, rotary_new)


def solution(mesh):
    return jax.shard_map(
        shards,
        mesh=mesh,
        in_specs=(
            P("ep", None),
            P("ep"),
            P("ep", None, None),
            P("ep", None, None),
            P("ep", None),
            P("ep", None),
            P(),
            P(),
            P(),
            P(),
            P(),
            P(),
            P(),
            P(),
            P(),
            P(),
            P(None, "ep"),
            P(),
            P("ep", None, None),
            P("ep", None, None),
            P("ep", None, None),
            P(),
            P(),
            P(),
        ),
        out_specs=(P("ep", None), P("ep", None), P("ep", None)),
        check_vma=False,
    )
```

profile of v0, /device:TPU:15, one launch (start us, length us, event | category | flops | bytes accessed | tf_op | source)
XLA Modules:
  0.0 229.1 jit_solution(12893498353833350144)
XLA Ops:
  7.3 0.7 all-gather.2.cloned.1.call-update
  8.0 0.7 convert_element_type.102
  8.6 0.7 convert_element_type.104
  9.3 1.0 fusion.55
  10.3 1.7 multiply_reduce_fusion.2
  12.0 1.3 fusion.77
  13.5 1.5 convolution_convert_fusion.2
  15.0 0.9 reshape.206
  16.4 1.6 multiply_reduce_fusion.1
  19.5 8.7 %fusion.50 = f32[24,32,1024]{2,1,0:T(8,128)S(1)} fusion(bf16[24,1024,256]{2,1,0:T(8,128)(2,1)} %param.26, bf16[24,32,256]{2,0,1:T(8,128)(2,1)S(1)} %fusion.32), kind=kOutput, calls=%fused_computation.50 | convolution fusion | flops 402653184 | bytes 16121856 | tf_op jit(solution)/shard_map/thl,tkl->thk/dot_general | solution.py:85
  28.2 2.6 %fusion.87 = (f32[24,32]{1,0:T(8,128)S(1)}, f32[24,32,1024]{2,1,0:T(8,128)S(1)}) fusion(f32[24,32,1024]{2,1,0:T(8,128)S(1)} %fusion.50, bf16[24,1024,32]{1,2,0:T(8,128)(2,1)} %param.27, bf16[24,32,16]{2,1,0:T(8,128)(2,1)S(1)} %get-tuple-element.6, bf16[24,32,16]{2,1,0:T(8,128)(2,1)S(1)} %get-tuple-element.5, pred[24,1024]{1,0:T(8,128)(4,1)S(1)} %iota_compare_fusion.2), kind=kOutput, calls=%fused_computation.118 | convolution fusion | flops 53574912 | bytes 7941120 | tf_op jit(solution)/shard_map/thr,tkr->thk/dot_general | solution.py:86
  30.8 0.7 fusion
  31.6 2.1 fusion.28
  33.7 0.5 fusion.33
  34.7 0.6 reduce-window.6
  35.9 52.7 %all-gather.2.cloned.1.call-done = bf16[2048,2048]{0,1:T(8,128)(2,1)} async-done(((bf16[2048,64]{0,1:T(8,128)(2,1)}), bf16[2048,2048]{0,1:T(8,128)(2,1)}) %all-gather.2.cloned.1.call-update) | async-done | bytes 8388624 | tf_op jit(solution)/shard_map/all_gather | solution.py:109
  88.6 5.8 %multiply_reduce_fusion = (f32[24]{0:T(128)S(1)}, f32[24,2048]{1,0:T(8,128)S(1)}) fusion(bf16[24,2048]{1,0:T(8,128)(2,1)S(1)} %reshape.208, bf16[2048,2048]{0,1:T(8,128)(2,1)} %all-gather.2.cloned.1.call-done, bf16[24,2048]{1,0:T(8,128)(2,1)S(1)} %copy-done.2), kind=kOutput, calls=%fused_computation.64 | convolution fusion | flops 201719776 | bytes 8781920 | tf_op jit(solution)/shard_map/dot_general | solution.py:108
  94.4 1.8 convolution_convert_fusion
  96.2 3.6 %reshape.211 = bf16[32,12,2048]{2,1,0:T(8,128)(2,1)} reshape(bf16[384,2048]{1,0:T(8,128)(2,1)} %convolution_convert_fusion) | data formatting | bytes 3145728 | tf_op jit(solution)/shard_map/reshape | solution.py:130
  99.8 49.9 %all_to_all.10 = bf16[32,12,2048]{2,1,0:T(8,128)(2,1)S(1)} all-to-all(bf16[32,12,2048]{2,1,0:T(8,128)(2,1)} %reshape.211), channel_id=1, replica_groups=mesh['ep'=32] {'ep'}, dimensions={0} | all-to-all | bytes 3145728 | tf_op jit(solution)/shard_map/all_to_all | solution.py:132
  149.7 1.3 copy-done.1
  151.0 1.1 fusion.14
  152.1 5.5 %convolution_convert_fusion.1 = bf16[32,12,2048]{2,0,1:T(8,128)(2,1)} fusion(bf16[1,512,2048]{2,1,0:T(8,128)(2,1)S(1)} %copy-done, bf16[1,2048,512]{2,1,0:T(8,128)(2,1)} %param.43, bf16[32,12,2048]{2,1,0:T(8,128)(2,1)} %copy-done.1, f32[32,1,12,512]{3,0,2,1:T(8,128)S(1)} %fusion.14), kind=kOutput, calls=%fused_computation.4 | convolution fusion | flops 1612578816 | bytes 8126464 | tf_op jit(solution)/shard_map/sjcf,jfd->sjcd/dot_general | solution.py:138
  157.6 3.6 %copy.78 = bf16[32,12,2048]{2,1,0:T(8,128)(2,1)} copy(bf16[32,12,2048]{2,0,1:T(8,128)(2,1)} %convolution_convert_fusion.1) | data formatting | bytes 3145728 | tf_op jit(solution)/shard_map/convert_element_type | solution.py:138
  161.2 6.7 %all-to-all-start.1 = ((bf16[32,12,2048]{2,1,0:T(8,128)(2,1)}), bf16[32,12,2048]{2,1,0:T(8,128)(2,1)}, u32[]{:S(2)}, u32[]{:S(2)}) async-start(bf16[32,12,2048]{2,1,0:T(8,128)(2,1)} %copy.78), calls=%async_computation.1 | async-start | bytes 4194304 | tf_op jit(solution)/shard_map/all_to_all | solution.py:141
  168.0 0.7 pad_maximum_fusion.3
  168.7 0.6 multiply_divide_fusion
  169.3 0.9 fusion.79
  170.2 43.9 %all-to-all-done.1 = bf16[32,12,2048]{2,1,0:T(8,128)(2,1)} async-done(((bf16[32,12,2048]{2,1,0:T(8,128)(2,1)}), bf16[32,12,2048]{2,1,0:T(8,128)(2,1)}, u32[]{:S(2)}, u32[]{:S(2)}) %all-to-all-start.1) | async-done | bytes 1572896 | tf_op jit(solution)/shard_map/all_to_all | solution.py:141
  214.0 3.6 %reshape.225 = bf16[384,2048,1]{1,0,2:T(8,128)(2,1)} reshape(bf16[32,12,2048]{2,1,0:T(8,128)(2,1)} %all-to-all-done.1) | data formatting | bytes 3145728 | tf_op jit(solution)/shard_map/reshape | solution.py:149
  217.6 1.9 fusion.24
  219.6 2.7 %fusion.1 = bf16[24,2048]{1,0:T(8,128)(2,1)} fusion(bf16[256,2048]{1,0:T(8,128)(2,1)S(1)} %copy-done.6, bf16[2048,256]{1,0:T(8,128)(2,1)} %param.46, f32[24,2048]{1,0:T(8,128)S(1)} %get-tuple-element.20, f32[24,2048]{1,0:T(8,128)S(1)} %fusion.24, f32[24,256]{1,0:T(8,128)} %fusion.79, f32[2048]{0:T(1024)S(1)} %convert_element_type.124, f32[24]{0:T(128)S(1)} %add_rsqrt_fusion), kind=kOutput, calls=%fused_computation.8 | convolution fusion | flops 50663424 | bytes 2621536 | tf_op jit(solution)/shard_map/dot_general | solution.py:156
  (75 shorter events, 3.3 us)
Async XLA Ops:
  7.2 145.0 %copy-start = (bf16[1,512,2048]{2,1,0:T(8,128)(2,1)S(1)}, bf16[1,512,2048]{2,1,0:T(8,128)(2,1)}, u32[]{:S(2)}) copy-start(bf16[1,512,2048]{2,1,0:T(8,128)(2,1)} %param.44) | copy-start | bytes 6291460
  7.2 8.7 %copy-start.2 = (bf16[24,2048]{1,0:T(8,128)(2,1)S(1)}, bf16[24,2048]{1,0:T(8,128)(2,1)}, u32[]{:S(2)}) copy-start(bf16[24,2048]{1,0:T(8,128)(2,1)} %param.24) | copy-start | bytes 294916
  7.2 6.3 %copy-start.12 = (s32[24]{0:T(128)S(1)}, s32[24]{0:T(128)}, u32[]{:S(2)}) copy-start(s32[24]{0:T(128)} %param.25) | copy-start | bytes 292
  7.2 8.7 %copy-start.15 = (bf16[256]{0:T(256)(128)(2,1)S(1)}, bf16[256]{0:T(256)(128)(2,1)}, u32[]{:S(2)}) copy-start(bf16[256]{0:T(256)(128)(2,1)} %param.36) | copy-start | bytes 1540
  7.2 8.7 %copy-start.14 = (bf16[2048,32]{0,1:T(8,128)(2,1)S(1)}, bf16[2048,32]{0,1:T(8,128)(2,1)}, u32[]{:S(2)}) copy-start(bf16[2048,32]{0,1:T(8,128)(2,1)} %param.38) | copy-start | bytes 393220
  7.2 81.4 %all-gather.2.cloned.1.call-start = ((), (), s32[]{:S(2)}) async-start(), calls=%async_computation.2 | async-start | bytes 8650752 | tf_op jit(solution)/shard_map/all_gather | solution.py:109
  15.9 2.8 %copy-start.3 = (bf16[32,64,256]{2,1,0:T(8,128)(2,1)S(1)}, bf16[32,64,256]{2,1,0:T(8,128)(2,1)}, u32[]{:S(2)}) copy-start(bf16[32,64,256]{2,1,0:T(8,128)(2,1)} %param.35) | copy-start | bytes 3145732
  15.9 2.8 %copy-start.7 = (bf16[24,32,64]{2,1,0:T(8,128)(2,1)S(1)}, bf16[24,32,64]{2,1,0:T(8,128)(2,1)}, u32[]{:S(2)}) copy-start(bf16[24,32,64]{2,1,0:T(8,128)(2,1)} %reshape.206) | copy-start | bytes 294916
  18.7 0.6 copy-start.10
  19.5 12.0 %slice-start = ((s8[12582912]{0:T(1024)(128)(4,1)}), s8[4194304]{0:T(1024)(128)(4,1)S(1)}, s32[]{:S(2)}) async-start(s8[12582912]{0:T(1024)(128)(4,1)} %bitcast.91), calls=%async_computation.3 | async-start | bytes 8388608
  19.5 12.1 %slice-start.1 = ((s8[12582912]{0:T(1024)(128)(4,1)}), s8[4194304]{0:T(1024)(128)(4,1)S(1)}, s32[]{:S(2)}) async-start(s8[12582912]{0:T(1024)(128)(4,1)} %bitcast.91), calls=%async_computation.4 | async-start | bytes 8388608
  28.2 3.3 %slice-start.2 = ((s8[12582912]{0:T(1024)(128)(4,1)}), s8[4194304]{0:T(1024)(128)(4,1)S(1)}, s32[]{:S(2)}) async-start(s8[12582912]{0:T(1024)(128)(4,1)} %bitcast.91), calls=%async_computation.5 | async-start | bytes 8388608
  31.6 2.1 copy-start.4
  33.7 0.8 copy-start.9
  33.7 2.1 copy-start.11
  99.8 51.2 %copy-start.13 = (bf16[1,2048,512]{2,1,0:T(8,128)(2,1)S(1)}, bf16[1,2048,512]{2,1,0:T(8,128)(2,1)}, u32[]{:S(2)}) copy-start(bf16[1,2048,512]{2,1,0:T(8,128)(2,1)} %param.42) | copy-start | bytes 6291460
  149.7 1.4 copy-start.1
  161.2 6.8 %copy-start.8 = (f32[24,6]{0,1:T(8,128)S(1)}, f32[24,6]{0,1:T(8,128)}, u32[]{:S(2)}) copy-start(f32[24,6]{0,1:T(8,128)} %param.29) | copy-start | bytes 1732
  161.2 8.1 %copy-start.5 = (bf16[2048,256]{1,0:T(8,128)(2,1)S(1)}, bf16[2048,256]{1,0:T(8,128)(2,1)}, u32[]{:S(2)}) copy-start(bf16[2048,256]{1,0:T(8,128)(2,1)} %param.45) | copy-start | bytes 3145732
  161.2 52.8 %all-to-all-start.1 = ((bf16[32,12,2048]{2,1,0:T(8,128)(2,1)}), bf16[32,12,2048]{2,1,0:T(8,128)(2,1)}, u32[]{:S(2)}, u32[]{:S(2)}) async-start(bf16[32,12,2048]{2,1,0:T(8,128)(2,1)} %copy.78), calls=%async_computation.1 | async-start | bytes 4194304 | tf_op jit(solution)/shard_map/all_to_all | solution.py:141
  170.2 49.4 %copy-start.6 = (bf16[256,2048]{1,0:T(8,128)(2,1)S(1)}, bf16[256,2048]{1,0:T(8,128)(2,1)}, u32[]{:S(2)}) copy-start(bf16[256,2048]{1,0:T(8,128)(2,1)} %param.47) | copy-start | bytes 3145732
Sparse Core Ops, SparseCore 0:
  10.9 77.6 all-gather.1
where the time goes:
time: 234 us; the launch traced here: 229 us
  waiting for transfers between devices  97.2 us (42%)
  blocking collectives  49.9 us (21%)
  matrix products  40.6 us (17%)
  local copies, waits for them, and re-layouts  14.4 us (6%)
  between operations  14.4 us (6%)
  starting transfers between devices  6.78 us (3%)
  other arithmetic  5.85 us (2%)
    all_gather x1, waiting for transfers between devices, shards(): lax.all_gather(w_output, 'ep', axis=1, tiled=True)  52.7 us
    all_to_all x1, blocking collectives, shards(): lax.all_to_all(outgoing, 'ep', split_axis=0, concat_axis=0, tiled=True)  49.9 us
    all_to_all x1, waiting for transfers between devices, shards(): lax.all_to_all(result.reshape(devices * local_experts, count, model), 'ep...  43.9 us
    dot_general x1, matrix products, shards(): jnp.einsum('thl,tkl->thk', query_lat, latent_cache, preferred_element_typ...  8.72 us
    all_to_all x1, starting transfers between devices, shards(): lax.all_to_all(result.reshape(devices * local_experts, count, model), 'ep...  6.75 us
    dot_general x1, matrix products, shards(): jnp.dot(values, lax.all_gather(w_output, 'ep', axis=1, tiled=True), prefe...  5.77 us
    dot_general x1, matrix products, shards(): jnp.einsum('sjcf,jfd->sjcd', hidden, expert_down, preferred_element_type=...  5.46 us
  transfers between devices with their start and end apart: 2, of which 2 were waited for; matrix products, arithmetic and copies ran while one was open for 13% of the time, Pallas kernels for 0%

commit v1 on v0

--- a/solution.py
+++ b/solution.py
@@ -57,7 +57,6 @@
     rows, model = tokens.shape
     heads, nope, latent = w_key_absorb.shape
     rotary = w_rotary_key.shape[1]
-    top = route_ids.shape[1]
     normed = rms_scale(tokens.astype(f32), attn_gain).astype(bf16)
     query_low = rms_scale(
         jnp.dot(normed, w_query_down, preferred_element_type=f32), query_gain
@@ -105,51 +104,36 @@
         bf16
     )
     values = values.reshape(rows, model)
-    attended = jnp.dot(
-        values, lax.all_gather(w_output, "ep", axis=1, tiled=True), preferred_element_type=f32
-    ).astype(bf16)
+    devices = lax.axis_size("ep")
+    me = lax.axis_index("ep")
+    local_experts = expert_gate.shape[0]
+    experts = devices * local_experts
+    route_weight = ROUTED_SCALE * route_scores / jnp.sum(route_scores, axis=1, keepdims=True)
+    chosen = route_ids[:, :, None] == jnp.arange(experts, dtype=jnp.int32)[None, None, :]
+    share = jnp.sum(jnp.where(chosen, route_weight[:, :, None], 0.0), axis=1)
+    share_high = share.astype(bf16)
+    share_low = (share - share_high.astype(f32)).astype(bf16)
+    packed = jnp.concatenate([values, share_high, share_low], axis=1)
+    everyone = lax.all_gather(packed, "ep", axis=0, tiled=True)
+    column_part = jnp.dot(everyone[:, :model], w_output, preferred_element_type=f32).astype(bf16)
+    attended = lax.all_to_all(column_part, "ep", split_axis=0, concat_axis=1, tiled=True)
     residual = (tokens.astype(f32) + attended.astype(f32)).astype(bf16)
     ffn_in = rms_scale(residual.astype(f32), ffn_gain).astype(bf16)
-    devices = lax.axis_size("ep")
-    local_experts = expert_gate.shape[0]
-    experts = devices * local_experts
-    capacity = max(2, rows * top * 8 // (3 * experts))
-    flat_ids = route_ids.reshape(-1)
-    hits = (flat_ids[:, None] == jnp.arange(experts, dtype=jnp.int32)[None, :]).astype(jnp.int32)
-    earlier = jnp.cumsum(hits, axis=0) - hits
-    slot = jnp.sum(earlier * hits, axis=1)
-    target = flat_ids * capacity + slot
-    slot_range = jnp.arange(experts * capacity, dtype=jnp.int32)
-    per_token = jnp.any(
-        slot_range[:, None, None] == target.reshape(rows, top)[None, :, :], axis=2
-    ).astype(bf16)
-    per_pair = (target[:, None] == slot_range[None, :]).astype(bf16)
-    outgoing = (
-        jnp.dot(per_token, ffn_in, preferred_element_type=f32)
-        .astype(bf16)
-        .reshape(experts, capacity, model)
-    )
-    arrived = lax.all_to_all(outgoing, "ep", split_axis=0, concat_axis=0, tiled=True)
-    count = arrived.shape[1]
-    grouped = arrived.reshape(devices, local_experts, count, model)
-    gate = jnp.einsum("sjcd,jdf->sjcf", grouped, expert_gate, preferred_element_type=f32)
-    upward = jnp.einsum("sjcd,jdf->sjcf", grouped, expert_up, preferred_element_type=f32)
-    hidden = (jax.nn.silu(gate) * upward).astype(bf16)
-    result = jnp.einsum("sjcf,jfd->sjcd", hidden, expert_down, preferred_element_type=f32).astype(
-        bf16
-    )
-    returned = lax.all_to_all(
-        result.reshape(devices * local_experts, count, model),
-        "ep",
-        split_axis=0,
-        concat_axis=0,
-        tiled=True,
-    )
-    picked = jnp.dot(
-        per_pair, returned.reshape(experts * capacity, model), preferred_element_type=f32
-    )
-    route_weight = ROUTED_SCALE * route_scores / jnp.sum(route_scores, axis=1, keepdims=True)
-    routed = jnp.sum(picked.reshape(rows, top, model) * route_weight[:, :, None], axis=1)
+    every_in = lax.all_gather(ffn_in, "ep", axis=0, tiled=True)
+    partial = jnp.zeros((devices * rows, model), f32)
+    for j in range(local_experts):
+        number = me * local_experts + j
+        weight = lax.dynamic_slice_in_dim(everyone, model + number, 1, 1).astype(
+            f32
+        ) + lax.dynamic_slice_in_dim(everyone, model + experts + number, 1, 1).astype(f32)
+        gate = jnp.dot(every_in, expert_gate[j], preferred_element_type=f32)
+        upward = jnp.dot(every_in, expert_up[j], preferred_element_type=f32)
+        hidden = (jax.nn.silu(gate) * upward).astype(bf16)
+        result = jnp.dot(hidden, expert_down[j], preferred_element_type=f32).astype(bf16)
+        partial = partial + result.astype(f32) * weight
+    routed = lax.psum_scatter(
+        partial.astype(bf16), "ep", scatter_dimension=0, tiled=True
+    ).astype(f32)
     gate_shared = jnp.dot(ffn_in, shared_gate, preferred_element_type=f32)
     up_shared = jnp.dot(ffn_in, shared_up, preferred_element_type=f32)
     hidden_shared = (jax.nn.silu(gate_shared) * up_shared).astype(bf16)

time: 234 us -> 295 us (1.26)
  waiting for transfers between devices: 97.2 us -> 219 us
  blocking collectives: 49.9 us -> 0 us
  local copies, waits for them, and re-layouts: 14.4 us -> 4.08 us
    reduce_scatter x0 -> x1, waiting for transfers between devices: none -> 99 us  [shards(): lax.psum_scatter(partial.astype(bf16), 'ep', scatter_dimension=0, tiled=T...]
    all_gather x1 -> x2, waiting for transfers between devices: 52.7 us -> 115 us  [the longest x1 59.4 us: shards(): everyone = lax.all_gather(packed, 'ep', axis=0, tiled=True)]
    all_to_all x1 -> x0, blocking collectives: 49.9 us -> none  [shards(): lax.all_to_all(outgoing, 'ep', split_axis=0, concat_axis=0, tiled=True)]
    all_to_all x1, waiting for transfers between devices: 43.9 us -> 4.86 us  [shards(): lax.all_to_all(column_part, 'ep', split_axis=0, concat_axis=1, tiled=True)]
    reshape x2 -> x0, local copies, waits for them, and re-layouts: 7.21 us -> none  [the longest x1 3.61 us: shards(): returned.reshape(experts * capacity, model)]
    convert_element_type x1 -> x3, local copies, waits for them, and re-layouts: 3.61 us -> 0.39 us  [the longest x2 0.22 us: shards(): residual = (tokens.astype(f32) + attended.astype(f32)).astype(bf16)]
    dot_general x5 -> x3, matrix products: 16.1 us -> 16.6 us  [the longest x1 8.17 us: shards(): jnp.dot(hidden, expert_down[j], preferred_element_type=f32).astype(bf16)]
  transfers between devices with their start and end apart: 2 -> 4, of which waited for: 2 -> 4; matrix products, arithmetic and copies ran while one was open for 13% -> 1% of each run, Pallas kernels for 0% -> 0%
where the time goes in v1:
time: 295 us; the launch traced here: 291 us
  waiting for transfers between devices  219 us (74%)
  matrix products  40.3 us (14%)
  between operations  14.1 us (5%)
  other arithmetic  8.22 us (3%)
  starting transfers between devices  5.66 us (2%)
  local copies, waits for them, and re-layouts  4.08 us (1%)
    reduce_scatter x1, waiting for transfers between devices, shards(): lax.psum_scatter(partial.astype(bf16), 'ep', scatter_dimension=0, tiled=T...  99 us
    all_gather x1, waiting for transfers between devices, shards(): everyone = lax.all_gather(packed, 'ep', axis=0, tiled=True)  59.4 us
    all_gather x1, waiting for transfers between devices, shards(): every_in = lax.all_gather(ffn_in, 'ep', axis=0, tiled=True)  55.4 us
    dot_general x1, matrix products, shards(): jnp.einsum('thl,tkl->thk', query_lat, latent_cache, preferred_element_typ...  8.46 us
    dot_general x1, matrix products, shards(): jnp.dot(hidden, expert_down[j], preferred_element_type=f32).astype(bf16)  8.17 us
  transfers between devices with their start and end apart: 4, of which 4 were waited for; matrix products, arithmetic and copies ran while one was open for 1% of the time, Pallas kernels for 0%

profile of v1, /device:TPU:15, one launch (start us, length us, event | category | flops | bytes accessed | tf_op | source)
XLA Modules:
  0.0 291.0 jit_solution(1610697426137891568)
XLA Ops:
  7.3 0.8 convert_element_type.127
  8.1 0.7 iota_compare_fusion
  8.8 0.7 convert_element_type.120
  9.5 1.0 fusion.29
  10.5 0.7 convert_element_type.122
  11.2 1.7 multiply_reduce_fusion.1
  12.9 1.5 convolution_convert_fusion.1
  14.6 1.3 fusion.52
  16.3 1.6 multiply_reduce_fusion
  17.9 1.5 fusion.16
  19.5 8.5 %fusion.27 = f32[24,32,1024]{2,1,0:T(8,128)S(1)} fusion(bf16[24,1024,256]{2,1,0:T(8,128)(2,1)} %param.26, bf16[24,32,256]{2,0,1:T(8,128)(2,1)S(1)} %fusion.16), kind=kOutput, calls=%fused_computation.36 | convolution fusion | flops 402653184 | bytes 16121856 | tf_op jit(solution)/shard_map/thl,tkl->thk/dot_general | solution.py:84
  29.0 0.4 copy-done.1
  29.4 1.1 fusion.66
  30.5 0.7 fusion.2
  31.2 0.4 slice-done.2
  31.6 2.1 fusion.15
  33.7 0.5 fusion.17
  34.6 0.7 concatenate.13
  35.3 59.4 %all-gather.3.cloned.1.call-done = bf16[768,2112]{1,0:T(8,128)(2,1)} async-done(((bf16[24,2112]{1,0:T(8,128)(2,1)}), bf16[768,2112]{1,0:T(8,128)(2,1)}) %all-gather.3.cloned.1.call-update) | async-done | bytes 3244048 | tf_op jit(solution)/shard_map/all_gather | solution.py:117
  94.7 3.0 %fusion.18 = bf16[768,64]{0,1:T(8,128)(2,1)S(1)} fusion(bf16[2048,64]{0,1:T(8,128)(2,1)S(1)} %copy-done.9, bf16[768,2112]{1,0:T(8,128)(2,1)} %all-gather.3.cloned.1.call-done), kind=kOutput, calls=%fused_computation.26 | convolution fusion | flops 201375744 | bytes 3506176 | tf_op jit(solution)/shard_map/dot_general | solution.py:118
  97.8 0.8 reshape.142
  98.7 5.4 %all-to-all-start = ((bf16[32,2,768]{2,1,0:T(2,128)(2,1)}), bf16[32,2,768]{2,1,0:T(2,128)(2,1)S(1)}, u32[]{:S(2)}, u32[]{:S(2)}) async-start(bf16[32,2,768]{2,1,0:T(2,128)(2,1)} %reshape.142), calls=%async_computation | async-start | bytes 196608 | tf_op jit(solution)/shard_map/all_to_all | solution.py:119
  104.1 4.9 %all-to-all-done = bf16[32,2,768]{2,1,0:T(2,128)(2,1)S(1)} async-done(((bf16[32,2,768]{2,1,0:T(2,128)(2,1)}), bf16[32,2,768]{2,1,0:T(2,128)(2,1)S(1)}, u32[]{:S(2)}, u32[]{:S(2)}) %all-to-all-start) | async-done | bytes 98336 | tf_op jit(solution)/shard_map/all_to_all | solution.py:119
  109.5 0.7 fusion.35
  110.5 1.3 add_reduce_fusion
  111.9 55.4 %all-gather.5.cloned.1.call-done = bf16[768,2048]{1,0:T(8,128)(2,1)} async-done(((bf16[24,2048]{1,0:T(8,128)(2,1)}), bf16[768,2048]{1,0:T(8,128)(2,1)}) %all-gather.5.cloned.1.call-update) | async-done | bytes 3145744 | tf_op jit(solution)/shard_map/all_gather | solution.py:122
  167.3 5.5 %fusion.7 = f32[768,512]{1,0:T(8,128)} fusion(bf16[768,2048]{1,0:T(8,128)(2,1)} %all-gather.5.cloned.1.call-done, bf16[1,2048,512]{2,1,0:T(8,128)(2,1)} %param.42), kind=kOutput, calls=%fused_computation.14 | convolution fusion | flops 1610612736 | bytes 6815744 | tf_op jit(solution)/shard_map/dot_general | solution.py:129
  172.8 8.2 %multiply_convert_fusion = bf16[768,2048]{1,0:T(8,128)(2,1)} fusion(f32[768]{0:T(1024)S(1)} %add_reduce_fusion, bf16[1,512,2048]{2,1,0:T(8,128)(2,1)S(1)} %copy-done, f32[768,512]{1,0:T(8,128)} %fusion.7, bf16[768,2048]{1,0:T(8,128)(2,1)} %all-gather.5.cloned.1.call-done, bf16[1,2048,512]{2,1,0:T(8,128)(2,1)} %param.43), kind=kOutput, calls=%fused_computation | convolution fusion | flops 3229876224 | bytes 12061696 | tf_op jit(solution)/shard_map/dot_general | solution.py:132
  181.0 0.7 pad_maximum_fusion.3
  181.6 0.5 copy-done.4
  182.4 99.0 %reduce-scatter.2.cloned.1.call-done = bf16[24,2048]{1,0:T(8,128)(2,1)} async-done(((bf16[768,2048]{1,0:T(8,128)(2,1)}), bf16[24,2048]{1,0:T(8,128)(2,1)}) %reduce-scatter.2.cloned.1.call-update) | async-done | bytes 98320 | tf_op jit(solution)/shard_map/reduce_scatter | solution.py:134
  281.5 3.0 %fusion.3 = bf16[24,2048]{1,0:T(8,128)(2,1)} fusion(bf16[256,2048]{1,0:T(8,128)(2,1)} %param.47, bf16[2048,256]{1,0:T(8,128)(2,1)} %param.46, bf16[24,2048]{1,0:T(8,128)(2,1)S(1)} %get-tuple-element.4, bf16[24,2048]{1,0:T(8,128)(2,1)} %reduce-scatter.2.cloned.1.call-done, f32[24,256]{1,0:T(8,128)S(1)} %fusion.62, f32[2048]{0:T(1024)S(1)} %convert_element_type.146, ...), kind=kOutput, calls=%fused_computation.9 | convolution fusion | flops 50810880 | bytes 2424928 | tf_op jit(solution)/shard_map/dot_general | solution.py:140
  (65 shorter events, 3.5 us)
Async XLA Ops:
  7.2 165.6 %copy-start = (bf16[1,512,2048]{2,1,0:T(8,128)(2,1)S(1)}, bf16[1,512,2048]{2,1,0:T(8,128)(2,1)}, u32[]{:S(2)}) copy-start(bf16[1,512,2048]{2,1,0:T(8,128)(2,1)} %param.44) | copy-start | bytes 6291460
  7.2 8.9 %copy-start.2 = (bf16[24,2048]{1,0:T(8,128)(2,1)S(1)}, bf16[24,2048]{1,0:T(8,128)(2,1)}, u32[]{:S(2)}) copy-start(bf16[24,2048]{1,0:T(8,128)(2,1)} %param.24) | copy-start | bytes 294916
  7.2 8.9 %copy-start.10 = (bf16[2048,32]{0,1:T(8,128)(2,1)S(1)}, bf16[2048,32]{0,1:T(8,128)(2,1)}, u32[]{:S(2)}) copy-start(bf16[2048,32]{0,1:T(8,128)(2,1)} %param.38) | copy-start | bytes 393220
  7.2 9.1 %copy-start.11 = (bf16[256]{0:T(256)(128)(2,1)S(1)}, bf16[256]{0:T(256)(128)(2,1)}, u32[]{:S(2)}) copy-start(bf16[256]{0:T(256)(128)(2,1)} %param.36) | copy-start | bytes 1540
  7.2 87.5 %all-gather.3.cloned.1.call-start = ((), (), s32[]{:S(2)}) async-start(), calls=%async_computation.2 | async-start | bytes 3446784 | tf_op jit(solution)/shard_map/all_gather | solution.py:117
  19.5 11.7 %slice-start = ((s8[12582912]{0:T(1024)(128)(4,1)}), s8[4194304]{0:T(1024)(128)(4,1)S(1)}, s32[]{:S(2)}) async-start(s8[12582912]{0:T(1024)(128)(4,1)} %bitcast.43), calls=%async_computation.5 | async-start | bytes 8388608
  19.5 11.7 %slice-start.1 = ((s8[12582912]{0:T(1024)(128)(4,1)}), s8[4194304]{0:T(1024)(128)(4,1)S(1)}, s32[]{:S(2)}) async-start(s8[12582912]{0:T(1024)(128)(4,1)} %bitcast.43), calls=%async_computation.6 | async-start | bytes 8388608
  28.0 1.4 copy-start.1
  28.1 2.4 copy-start.6
  29.4 2.2 slice-start.2
  31.6 2.1 copy-start.3
  31.6 2.8 copy-start.5
  31.6 2.9 copy-start.7
  31.6 63.1 %copy-start.9 = (bf16[2048,64]{0,1:T(8,128)(2,1)S(1)}, bf16[2048,64]{0,1:T(8,128)(2,1)}, u32[]{:S(2)}) copy-start(bf16[2048,64]{0,1:T(8,128)(2,1)} %param.40) | copy-start | bytes 786436
  35.3 68.7 %copy-start.8 = (bf16[2048]{0:T(1024)(128)(2,1)S(1)}, bf16[2048]{0:T(1024)(128)(2,1)}, u32[]{:S(2)}) copy-start(bf16[2048]{0:T(1024)(128)(2,1)} %param.41) | copy-start | bytes 12292
  98.7 10.3 %all-to-all-start = ((bf16[32,2,768]{2,1,0:T(2,128)(2,1)}), bf16[32,2,768]{2,1,0:T(2,128)(2,1)S(1)}, u32[]{:S(2)}, u32[]{:S(2)}) async-start(bf16[32,2,768]{2,1,0:T(2,128)(2,1)} %reshape.142), calls=%async_computation | async-start | bytes 196608 | tf_op jit(solution)/shard_map/all_to_all | solution.py:119
  104.0 63.3 %all-gather.5.cloned.1.call-start = ((), (), s32[]{:S(2)}) async-start(), calls=%async_computation.3 | async-start | bytes 3244032 | tf_op jit(solution)/shard_map/all_gather | solution.py:122
  110.3 171.2 %reduce-scatter.2.cloned.1.call-start = ((), (), s32[]{:S(2)}) async-start(), calls=%async_computation.4 | async-start | bytes 3244032 | tf_op jit(solution)/shard_map/reduce_scatter | solution.py:134
  180.9 1.2 copy-start.4
Sparse Core Ops, SparseCore 0:
  35.5 59.2 all-gather.2
  110.4 56.8 all-gather.4
  181.1 100.3 reduce-scatter.1

commit v2 on v0

--- a/solution.py
+++ b/solution.py
@@ -1,6 +1,8 @@
 import jax
 import jax.numpy as jnp
 from jax import lax
+from jax.experimental import pallas as pl
+from jax.experimental.pallas import tpu as pltpu
 from jax.sharding import PartitionSpec as P
 
 EPSILON = 1e-06
@@ -24,6 +26,75 @@
     return jnp.concatenate(
         [first * cosine - second * sine, second * cosine + first * sine], axis=-1
     )
+
+
+def exchange_kernel(n, src, dst, send_sem, recv_sem, local_sem):
+    me = lax.axis_index("ep")
+    barrier = pltpu.get_barrier_semaphore()
+
+    def greet(i, carry):
+        pl.semaphore_signal(
+            barrier,
+            inc=1,
+            device_id=(lax.rem(me + i, n),),
+            device_id_type=pl.DeviceIdType.MESH,
+        )
+        return carry
+
+    lax.fori_loop(1, n, greet, 0)
+    pl.semaphore_wait(barrier, n - 1)
+    own = pltpu.make_async_copy(src.at[me], dst.at[me], local_sem)
+    own.start()
+
+    def send(i, carry):
+        peer = lax.rem(me + i, n)
+        pltpu.make_async_remote_copy(
+            src_ref=src.at[peer],
+            dst_ref=dst.at[me],
+            send_sem=send_sem.at[i],
+            recv_sem=recv_sem.at[i],
+            device_id=(peer,),
+            device_id_type=pl.DeviceIdType.MESH,
+        ).start()
+        return carry
+
+    lax.fori_loop(1, n, send, 0)
+
+    def finish(i, carry):
+        peer = lax.rem(me + i, n)
+        sender = lax.rem(me + n - i, n)
+        copy = pltpu.make_async_remote_copy(
+            src_ref=src.at[peer],
+            dst_ref=dst.at[sender],
+            send_sem=send_sem.at[i],
+            recv_sem=recv_sem.at[i],
+            device_id=(peer,),
+            device_id_type=pl.DeviceIdType.MESH,
+        )
+        copy.wait_send()
+        copy.wait_recv()
+        return carry
+
+    lax.fori_loop(1, n, finish, 0)
+    own.wait()
+
+
+def exchange(blocks, number):
+    n = blocks.shape[0]
+    dense = blocks.reshape(n, -1, 128)
+    return pl.pallas_call(
+        lambda *refs: exchange_kernel(n, *refs),
+        out_shape=jax.ShapeDtypeStruct(dense.shape, dense.dtype),
+        in_specs=[pl.BlockSpec(memory_space=pltpu.VMEM)],
+        out_specs=pl.BlockSpec(memory_space=pltpu.VMEM),
+        scratch_shapes=[
+            pltpu.SemaphoreType.DMA((n,)),
+            pltpu.SemaphoreType.DMA((n,)),
+            pltpu.SemaphoreType.DMA,
+        ],
+        compiler_params=pltpu.CompilerParams(collective_id=number, has_side_effects=True),
+        name=("dispatch", "combine")[number],
+    )(dense).reshape(blocks.shape)
 
 
 def shards(
@@ -129,8 +200,8 @@
         .astype(bf16)
         .reshape(experts, capacity, model)
     )
-    arrived = lax.all_to_all(outgoing, "ep", split_axis=0, concat_axis=0, tiled=True)
-    count = arrived.shape[1]
+    count = capacity
+    arrived = exchange(outgoing.reshape(devices, local_experts * count, model), 0)
     grouped = arrived.reshape(devices, local_experts, count, model)
     gate = jnp.einsum("sjcd,jdf->sjcf", grouped, expert_gate, preferred_element_type=f32)
     upward = jnp.einsum("sjcd,jdf->sjcf", grouped, expert_up, preferred_element_type=f32)
@@ -138,13 +209,7 @@
     result = jnp.einsum("sjcf,jfd->sjcd", hidden, expert_down, preferred_element_type=f32).astype(
         bf16
     )
-    returned = lax.all_to_all(
-        result.reshape(devices * local_experts, count, model),
-        "ep",
-        split_axis=0,
-        concat_axis=0,
-        tiled=True,
-    )
+    returned = exchange(result.reshape(devices, local_experts * count, model), 1)
     picked = jnp.dot(
         per_pair, returned.reshape(experts * capacity, model), preferred_element_type=f32
     )

time: 234 us -> 224 us (0.957); the launches traced: 229 us -> 223 us
  Pallas kernels: 0 us -> 86.3 us
  blocking collectives: 49.9 us -> 0 us
  waiting for transfers between devices: 97.2 us -> 51.9 us
  local copies, waits for them, and re-layouts: 14.4 us -> 21.3 us
  starting transfers between devices: 6.78 us -> 0.04 us
    pallas_call x0 -> x2, Pallas kernels: none -> 86.3 us  [exchange(): pl.pallas_call(lambda *refs: exchange_kernel(n, *refs), out_shape=jax.Sha...]
    all_to_all x1 -> x0, blocking collectives: 49.9 us -> none  [shards(): lax.all_to_all(outgoing, 'ep', split_axis=0, concat_axis=0, tiled=True)]
    all_to_all x1 -> x0, waiting for transfers between devices: 43.9 us -> none  [shards(): lax.all_to_all(result.reshape(devices * local_experts, count, model), 'ep...]
    another operation x1 -> x5, local copies, waits for them, and re-layouts: 0.01 us -> 15.5 us  [the longest x2 7.67 us: exchange(): dense = blocks.reshape(n, -1, 128)]
    reshape x2 -> x0, local copies, waits for them, and re-layouts: 7.21 us -> none  [the longest x1 3.61 us: shards(): returned.reshape(experts * capacity, model)]
    all_to_all x1 -> x0, starting transfers between devices: 6.75 us -> none  [shards(): lax.all_to_all(result.reshape(devices * local_experts, count, model), 'ep...]
  transfers between devices with their start and end apart: 2 -> 1, of which waited for: 2 -> 1; matrix products, arithmetic and copies ran while one was open for 13% -> 13% of each run, Pallas kernels for 0% -> 0%
where the time goes in v2:
time: 224 us; the launch traced here: 223 us
  Pallas kernels  86.3 us (39%)
  waiting for transfers between devices  51.9 us (23%)
  matrix products  42.8 us (19%)
  local copies, waits for them, and re-layouts  21.3 us (10%)
  between operations  14.4 us (6%)
  other arithmetic  6.03 us (3%)
    pallas_call x2, Pallas kernels, exchange(): pl.pallas_call(lambda *refs: exchange_kernel(n, *refs), out_shape=jax.Sha...  86.3 us
    all_gather x1, waiting for transfers between devices, shards(): lax.all_gather(w_output, 'ep', axis=1, tiled=True)  51.2 us
    dot_general x1, matrix products, shards(): jnp.einsum('thl,tkl->thk', query_lat, latent_cache, preferred_element_typ...  8.72 us
    another operation x2, local copies, waits for them, and re-layouts, exchange(): dense = blocks.reshape(n, -1, 128)  7.67 us
    dot_general x1, matrix products, shards(): jnp.dot(values, lax.all_gather(w_output, 'ep', axis=1, tiled=True), prefe...  5.77 us
    dot_general x1, matrix products, shards(): jnp.einsum('sjcf,jfd->sjcd', hidden, expert_down, preferred_element_type=...  5.42 us
  transfers between devices with their start and end apart: 1, of which 1 were waited for; matrix products, arithmetic and copies ran while one was open for 13% of the time, Pallas kernels for 0%

profile of v2, /device:TPU:15, one launch (start us, length us, event | category | flops | bytes accessed | tf_op | source)
XLA Modules:
  0.0 222.8 jit_solution(18140264201356457901)
XLA Ops:
  7.3 0.7 all-gather.2.cloned.1.call-update
  8.0 0.7 convert_element_type.108
  8.6 0.7 convert_element_type.110
  9.3 1.0 fusion.51
  10.3 1.7 multiply_reduce_fusion.2
  12.0 1.3 fusion.73
  13.5 1.5 convolution_convert_fusion.2
  15.0 0.9 reshape.200
  16.4 1.6 multiply_reduce_fusion.1
  19.5 8.7 %fusion.46 = f32[24,32,1024]{2,1,0:T(8,128)S(1)} fusion(bf16[24,1024,256]{2,1,0:T(8,128)(2,1)} %param.26, bf16[24,32,256]{2,0,1:T(8,128)(2,1)S(1)} %fusion.33), kind=kOutput, calls=%fused_computation.46 | convolution fusion | flops 402653184 | bytes 16121856 | tf_op jit(solution)/shard_map/thl,tkl->thk/dot_general | solution.py:156
  28.2 2.6 %fusion.83 = (f32[24,32]{1,0:T(8,128)S(1)}, f32[24,32,1024]{2,1,0:T(8,128)S(1)}) fusion(f32[24,32,1024]{2,1,0:T(8,128)S(1)} %fusion.46, bf16[24,1024,32]{1,2,0:T(8,128)(2,1)} %param.27, bf16[24,32,16]{2,1,0:T(8,128)(2,1)S(1)} %get-tuple-element.6, bf16[24,32,16]{2,1,0:T(8,128)(2,1)S(1)} %get-tuple-element.5, pred[24,1024]{1,0:T(8,128)(4,1)S(1)} %iota_compare_fusion.2), kind=kOutput, calls=%fused_computation.114 | convolution fusion | flops 53574912 | bytes 7941120 | tf_op jit(solution)/shard_map/thr,tkr->thk/dot_general | solution.py:157
  30.8 0.7 fusion
  31.6 2.1 fusion.29
  33.7 0.5 fusion.34
  34.7 0.8 reduce-window.6
  36.0 0.7 pad_maximum_fusion.3
  36.8 0.6 multiply_divide_fusion
  37.4 51.2 %all-gather.2.cloned.1.call-done = bf16[2048,2048]{0,1:T(8,128)(2,1)} async-done(((bf16[2048,64]{0,1:T(8,128)(2,1)}), bf16[2048,2048]{0,1:T(8,128)(2,1)}) %all-gather.2.cloned.1.call-update) | async-done | bytes 8388624 | tf_op jit(solution)/shard_map/all_gather | solution.py:180
  88.6 5.8 %multiply_reduce_fusion = (f32[24]{0:T(128)S(1)}, f32[24,2048]{1,0:T(8,128)S(1)}) fusion(bf16[24,2048]{1,0:T(8,128)(2,1)S(1)} %reshape.202, bf16[2048,2048]{0,1:T(8,128)(2,1)} %all-gather.2.cloned.1.call-done, bf16[24,2048]{1,0:T(8,128)(2,1)S(1)} %copy-done.1), kind=kOutput, calls=%fused_computation.60 | convolution fusion | flops 201719776 | bytes 8781920 | tf_op jit(solution)/shard_map/dot_general | solution.py:179
  94.4 1.8 convolution_convert_fusion
  96.2 3.8 %reshape_reshape.10.refs_0_ = bf16[32,192,128]{2,1,0:T(8,128)(2,1)} reshape(bf16[384,2048]{1,0:T(8,128)(2,1)} %convolution_convert_fusion) | data formatting | bytes 3145728 | tf_op jit(solution)/shard_map/reshape;reshape | solution.py:84
  99.9 43.7 %dispatch.1 = bf16[32,192,128]{2,1,0:T(8,128)(2,1)} custom-call(bf16[32,192,128]{2,1,0:T(8,128)(2,1)} %reshape_reshape.10.refs_0_), custom_call_target="tpu_custom_call" | custom-call | tf_op jit(solution)/shard_map/dispatch/pallas_call | solution.py:85
  143.7 4.0 %reshape.205 = bf16[32,12,2048]{2,1,0:T(8,128)(2,1)} reshape(bf16[32,192,128]{2,1,0:T(8,128)(2,1)} %dispatch.1) | data formatting | bytes 3145728 | tf_op jit(solution)/shard_map/reshape.4
  147.7 3.3 %fusion.15 = f32[32,1,12,512]{3,0,2,1:T(8,128)S(1)} fusion(bf16[1,2048,512]{2,1,0:T(8,128)(2,1)} %param.42, bf16[32,12,2048]{2,1,0:T(8,128)(2,1)} %reshape.205), kind=kOutput, calls=%fused_computation.24 | convolution fusion | flops 805306368 | bytes 4456448 | tf_op jit(solution)/shard_map/sjcd,jdf->sjcf/dot_general | solution.py:206
  151.0 5.4 %fusion.1 = bf16[32,1,12,2048]{3,0,2,1:T(8,128)(2,1)} fusion(bf16[1,512,2048]{2,1,0:T(8,128)(2,1)S(1)} %copy-done, bf16[1,2048,512]{2,1,0:T(8,128)(2,1)} %param.43, bf16[32,12,2048]{2,1,0:T(8,128)(2,1)} %reshape.205, f32[32,1,12,512]{3,0,2,1:T(8,128)S(1)} %fusion.15), kind=kOutput, calls=%fused_computation.6 | convolution fusion | flops 1612578816 | bytes 8126464 | tf_op jit(solution)/shard_map/sjcf,jfd->sjcd/dot_general | solution.py:209
  156.4 3.7 %copy.69 = bf16[32,1,12,2048]{3,2,0,1:T(8,128)(2,1)} copy(bf16[32,1,12,2048]{3,0,2,1:T(8,128)(2,1)} %fusion.1) | data formatting | bytes 3145728 | tf_op jit(solution)/shard_map/convert_element_type | solution.py:209
  160.1 3.9 %reshape_reshape.11.refs_0_ = bf16[32,192,128]{2,1,0:T(8,128)(2,1)} reshape(bf16[32,1,12,2048]{3,2,0,1:T(8,128)(2,1)} %copy.69) | data formatting | bytes 3145728 | tf_op jit(solution)/shard_map/reshape;reshape | solution.py:84
  164.0 42.6 %combine.1 = bf16[32,192,128]{2,1,0:T(8,128)(2,1)} custom-call(bf16[32,192,128]{2,1,0:T(8,128)(2,1)} %reshape_reshape.11.refs_0_), custom_call_target="tpu_custom_call" | custom-call | tf_op jit(solution)/shard_map/combine/pallas_call | solution.py:85
  206.6 3.8 %reshape.218 = bf16[384,2048,1]{1,0,2:T(8,128)(2,1)} reshape(bf16[32,192,128]{2,1,0:T(8,128)(2,1)} %combine.1) | data formatting | bytes 3145728 | tf_op jit(solution)/shard_map/reshape;reshape | solution.py:214
  210.4 0.9 fusion.75
  211.2 2.0 fusion.25
  213.3 2.7 %fusion.2 = bf16[24,2048]{1,0:T(8,128)(2,1)} fusion(bf16[256,2048]{1,0:T(8,128)(2,1)S(1)} %copy-done.5, bf16[2048,256]{1,0:T(8,128)(2,1)} %param.46, f32[24,2048]{1,0:T(8,128)S(1)} %get-tuple-element.20, f32[24,2048]{1,0:T(8,128)S(1)} %fusion.25, f32[24,256]{1,0:T(8,128)} %fusion.75, f32[2048]{0:T(1024)S(1)} %convert_element_type.130, f32[24]{0:T(128)S(1)} %add_rsqrt_fusion), kind=kOutput, calls=%fused_computation.9 | convolution fusion | flops 50663424 | bytes 2621536 | tf_op jit(solution)/shard_map/dot_general | solution.py:221
  (72 shorter events, 3.3 us)
Async XLA Ops:
  7.2 143.8 %copy-start = (bf16[1,512,2048]{2,1,0:T(8,128)(2,1)S(1)}, bf16[1,512,2048]{2,1,0:T(8,128)(2,1)}, u32[]{:S(2)}) copy-start(bf16[1,512,2048]{2,1,0:T(8,128)(2,1)} %param.44) | copy-start | bytes 6291460
  7.2 8.7 %copy-start.1 = (bf16[24,2048]{1,0:T(8,128)(2,1)S(1)}, bf16[24,2048]{1,0:T(8,128)(2,1)}, u32[]{:S(2)}) copy-start(bf16[24,2048]{1,0:T(8,128)(2,1)} %param.24) | copy-start | bytes 294916
  7.2 6.3 %copy-start.11 = (s32[24]{0:T(128)S(1)}, s32[24]{0:T(128)}, u32[]{:S(2)}) copy-start(s32[24]{0:T(128)} %param.25) | copy-start | bytes 292
  7.2 8.7 %copy-start.13 = (bf16[256]{0:T(256)(128)(2,1)S(1)}, bf16[256]{0:T(256)(128)(2,1)}, u32[]{:S(2)}) copy-start(bf16[256]{0:T(256)(128)(2,1)} %param.36) | copy-start | bytes 1540
  7.2 8.7 %copy-start.12 = (bf16[2048,32]{0,1:T(8,128)(2,1)S(1)}, bf16[2048,32]{0,1:T(8,128)(2,1)}, u32[]{:S(2)}) copy-start(bf16[2048,32]{0,1:T(8,128)(2,1)} %param.38) | copy-start | bytes 393220
  7.2 81.4 %all-gather.2.cloned.1.call-start = ((), (), s32[]{:S(2)}) async-start(), calls=%async_computation | async-start | bytes 8650752 | tf_op jit(solution)/shard_map/all_gather | solution.py:180
  15.9 2.8 %copy-start.2 = (bf16[32,64,256]{2,1,0:T(8,128)(2,1)S(1)}, bf16[32,64,256]{2,1,0:T(8,128)(2,1)}, u32[]{:S(2)}) copy-start(bf16[32,64,256]{2,1,0:T(8,128)(2,1)} %param.35) | copy-start | bytes 3145732
  15.9 2.8 %copy-start.6 = (bf16[24,32,64]{2,1,0:T(8,128)(2,1)S(1)}, bf16[24,32,64]{2,1,0:T(8,128)(2,1)}, u32[]{:S(2)}) copy-start(bf16[24,32,64]{2,1,0:T(8,128)(2,1)} %reshape.200) | copy-start | bytes 294916
  18.7 0.6 copy-start.9
  19.5 12.0 %slice-start = ((s8[12582912]{0:T(1024)(128)(4,1)}), s8[4194304]{0:T(1024)(128)(4,1)S(1)}, s32[]{:S(2)}) async-start(s8[12582912]{0:T(1024)(128)(4,1)} %bitcast.99), calls=%async_computation.1 | async-start | bytes 8388608
  19.5 12.1 %slice-start.1 = ((s8[12582912]{0:T(1024)(128)(4,1)}), s8[4194304]{0:T(1024)(128)(4,1)S(1)}, s32[]{:S(2)}) async-start(s8[12582912]{0:T(1024)(128)(4,1)} %bitcast.99), calls=%async_computation.2 | async-start | bytes 8388608
  28.2 3.3 %slice-start.2 = ((s8[12582912]{0:T(1024)(128)(4,1)}), s8[4194304]{0:T(1024)(128)(4,1)S(1)}, s32[]{:S(2)}) async-start(s8[12582912]{0:T(1024)(128)(4,1)} %bitcast.99), calls=%async_computation.3 | async-start | bytes 8388608
  31.6 2.1 copy-start.3
  33.7 0.8 copy-start.8
  33.7 2.3 %copy-start.10 = (bf16[2048]{0:T(1024)(128)(2,1)S(1)}, bf16[2048]{0:T(1024)(128)(2,1)}, u32[]{:S(2)}) copy-start(bf16[2048]{0:T(1024)(128)(2,1)} %param.41) | copy-start | bytes 12292
  33.7 2.3 %copy-start.7 = (f32[24,6]{0,1:T(8,128)S(1)}, f32[24,6]{0,1:T(8,128)}, u32[]{:S(2)}) copy-start(f32[24,6]{0,1:T(8,128)} %param.29) | copy-start | bytes 1732
  206.5 3.8 %copy-start.4 = (bf16[2048,256]{1,0:T(8,128)(2,1)S(1)}, bf16[2048,256]{1,0:T(8,128)(2,1)}, u32[]{:S(2)}) copy-start(bf16[2048,256]{1,0:T(8,128)(2,1)} %param.45) | copy-start | bytes 3145732
  211.2 2.0 copy-start.5
Sparse Core Ops, SparseCore 0:
  10.9 77.6 all-gather.1
